TPU v7x, 32 devices: a whole 2x2x4 slice. The times are simulated.
32 devices in a mesh: sp: 16 (over z, y, core), tp: 2 (over x).
Axes of the slice: x: 2, y: 2, z: 4, core: 2. Of those that a mesh axis runs over, the one named last changes fastest.
Arguments:
- tokens_in: bfloat16 [4096, 2048], P('sp', 'tp'), may hold values from -400 to 400
- norm_gain: float32 [2048], replicated, may hold values from 0.1 to 1.9
- w_query: bfloat16 [2048, 1024], P('sp', 'tp'), may hold values from -0.125 to 0.125
- w_forget: bfloat16 [2048, 1024], P('sp', 'tp'), may hold values from -0.125 to 0.125
- w_input: bfloat16 [2048, 1024], P('sp', 'tp'), may hold values from -0.125 to 0.125
- w_rgate: bfloat16 [2048, 1024], P('sp', 'tp'), may hold values from -0.125 to 0.125
- w_pool_in: bfloat16 [2048, 1024], P('sp', 'tp'), may hold values from -0.125 to 0.125
- w_pgate: bfloat16 [2048, 1024], P('sp', 'tp'), may hold values from -0.125 to 0.125
- floor_rate: float32 [1024], P('tp'), as said below
- extra_logdecay: float32 [4096, 8], P('sp', 'tp'), as said below
- state_gain: float32 [1024], P('tp'), may hold values from 0.1 to 1.9
- pool_mix: bfloat16 [8, 128, 128], P('tp'), may hold values from -0.5 to 0.5
- pool_gain: float32 [1024], P('tp'), may hold values from 0.1 to 1.9
- out_rec: bfloat16 [1024, 2048], P('tp', 'sp'), may hold values from -0.125 to 0.125
- out_pool: bfloat16 [1024, 2048], P('tp', 'sp'), may hold values from -0.125 to 0.125
- post_gain: float32 [2048], replicated, may hold values from 0.1 to 1.9
Outputs:
- mixed_out: bfloat16 [4096, 2048], P(('sp', 'tp'))
Inputs may be any that keep to these rules, and one draw needn't show every extreme that they name: `floor_rate`: every entry is positive. `extra_logdecay`: every entry is at most zero.
All inputs are finite; a program needn't handle non-finite values.
Results may differ from a plain program's by a relative error of at most 0.015.
Values may be sent and summed in bfloat16 or wider, within the bound.
A program may use at most 64 MiB of HBM per device.

v0:
```python
import jax
import jax.numpy as jnp
from jax import lax
from jax.sharding import PartitionSpec as P

DK = 128
BLOCK = 64
eps = 1e-06
coarsest_scale_depth = lax.Precision.HIGHEST


def prefix(part, axis, combine, identity):
    place = lax.axis_index(axis)
    gathered = jax.tree.map(lambda a: lax.all_gather(a, axis), part)
    state = jax.tree.map(lambda a, e: jnp.zeros_like(a) + jnp.asarray(e, a.dtype), part, identity)

    def one(turn, state):
        return combine(
            state, jax.tree.map(lambda a: lax.dynamic_index_in_dim(a, turn, 0, False), gathered)
        )

    return lax.fori_loop(0, place, one, state)


def shifted(value, axis, steps):
    count = lax.axis_size(axis)
    initial, last = (max(0, -steps), min(count, count - steps))
    return lax.ppermute(value, axis, [(source, source + steps) for source in range(initial, last)])


def chain_merge(earlier, later):
    return (earlier[0] * later[0], later[0][..., None] * earlier[1] + later[1])


def local_blocks(qs, keys, values, logs):
    causal = jnp.arange(BLOCK)[:, None] >= jnp.arange(BLOCK)[None, :]
    heads_dev = qs.shape[1]

    def advance(carry, member):
        carried_memory_matrix, start = carry
        probe_segment, key_piece, input_piece, gc = member
        prefix_sum_vector = jnp.cumsum(gc, axis=1)
        last_index = prefix_sum_vector[:, -1]
        cross_segment_contribution = jnp.einsum(
            "abz,azy->aby",
            probe_segment * jnp.exp(prefix_sum_vector),
            carried_memory_matrix,
            precision=coarsest_scale_depth,
        )
        diff = prefix_sum_vector[:, :, None, :] - prefix_sum_vector[:, None, :, :]
        weight = jnp.where(causal[None, :, :, None], jnp.exp(jnp.minimum(diff, 0.0)), 0.0)
        scores = jnp.einsum(
            "htk,hsk,htsk->hts", probe_segment, key_piece, weight, precision=coarsest_scale_depth
        )
        final_result = cross_segment_contribution + jnp.einsum(
            "hts,hsv->htv", scores, input_piece, precision=coarsest_scale_depth
        )
        carried_memory_matrix = jnp.exp(last_index)[..., None] * carried_memory_matrix + jnp.einsum(
            "njp,njq->npq",
            key_piece * jnp.exp(last_index[:, None, :] - prefix_sum_vector),
            input_piece,
            precision=coarsest_scale_depth,
        )
        pool_reach = probe_segment * jnp.exp(start[:, None, :] + prefix_sum_vector)
        return ((carried_memory_matrix, start + last_index), (final_result, pool_reach))

    begin = (jnp.zeros((heads_dev, DK, DK), jnp.float32), jnp.zeros((heads_dev, DK), jnp.float32))
    (carried_memory_matrix, total), (final_result, pool_reach) = lax.scan(
        advance, begin, (qs, keys, values, logs)
    )
    return (carried_memory_matrix, total, final_result, pool_reach)


def per_device(
    tokens_in,
    norm_gain,
    w_query,
    w_forget,
    w_input,
    w_rgate,
    w_pool_in,
    w_pgate,
    floor_rate,
    extra_logdecay,
    state_gain,
    pool_mix,
    pool_gain,
    out_rec,
    out_pool,
    post_gain,
):
    gathered = (
        lax.all_gather(w_query, "sp", axis=0, tiled=True),
        lax.all_gather(w_forget, "sp", axis=0, tiled=True),
        lax.all_gather(w_input, "sp", axis=0, tiled=True),
        lax.all_gather(w_rgate, "sp", axis=0, tiled=True),
        lax.all_gather(w_pool_in, "sp", axis=0, tiled=True),
        lax.all_gather(w_pgate, "sp", axis=0, tiled=True),
    )
    joined = jnp.concatenate(gathered, axis=1)
    head_cols = w_query.shape[1]
    positions = tokens_in.shape[0]
    model_width = norm_gain.shape[0]
    wide = lax.all_gather(tokens_in, "tp", axis=1, tiled=True).astype(jnp.float32)
    scaled = (wide * norm_gain[None, :]).astype(jnp.bfloat16)
    totals = jnp.dot(scaled, joined, preferred_element_type=jnp.float32)
    squares = jnp.sum(wide * wide, axis=1)
    inv_rms = lax.rsqrt(squares / model_width + eps)
    proj = (totals * inv_rms[:, None]).astype(jnp.bfloat16)
    query = proj[:, 0:head_cols]
    forget = proj[:, head_cols : 2 * head_cols]
    inputs = proj[:, 2 * head_cols : 3 * head_cols]
    rgate = proj[:, 3 * head_cols : 4 * head_cols]
    pool_in = proj[:, 4 * head_cols : 5 * head_cols]
    pgate = proj[:, 5 * head_cols : 6 * head_cols]
    heads_dev = head_cols // DK
    blocks = positions // BLOCK

    def to_blocks(array):
        return array.reshape(blocks, BLOCK, heads_dev, DK).transpose(0, 2, 1, 3)

    forget32 = forget.astype(jnp.float32)
    key_gate = -jnp.expm1(-floor_rate)[None, :] * jax.nn.sigmoid(-forget32)
    log_forget = jnp.log1p(-key_gate) + jnp.repeat(extra_logdecay, DK, axis=1)
    qs = query.astype(jnp.float32) * DK ** (-0.5)
    carried_memory_matrix, total, final_result, pool_reach = local_blocks(
        to_blocks(qs),
        to_blocks(key_gate),
        to_blocks(inputs.astype(jnp.float32)),
        to_blocks(log_forget),
    )
    decays = jnp.exp(total)
    tail_rows = pool_in[positions - 16 :]
    carried = prefix(
        (decays, carried_memory_matrix),
        "sp",
        chain_merge,
        (jnp.ones_like(decays), jnp.zeros_like(carried_memory_matrix)),
    )
    incoming_state = carried[1]
    previous = shifted(tail_rows, "sp", 1).astype(jnp.float32)
    recurrent_output = final_result + jnp.einsum(
        "izaf,zfu->izau", pool_reach, incoming_state, precision=coarsest_scale_depth
    )
    grouped = recurrent_output.transpose(0, 2, 1, 3).reshape(positions, heads_dev, DK)
    normed = grouped * lax.rsqrt(jnp.mean(grouped * grouped, axis=2, keepdims=True) + eps)
    y_rec = (
        normed.reshape(positions, head_cols)
        * state_gain[None, :]
        * jax.nn.silu(rgate.astype(jnp.float32))
    ).astype(jnp.bfloat16)
    group = lax.axis_index("tp") * heads_dev + jnp.arange(head_cols) // DK
    window = jnp.power(2, 1 + group % 4).astype(jnp.int32)
    pool32 = pool_in.astype(jnp.float32)
    extended = jnp.concatenate([previous, pool32], axis=0)
    summed_rows = jnp.zeros((positions, head_cols), jnp.float32)
    for offset in range(16):
        rows_back = extended[16 - offset : 16 - offset + positions]
        summed_rows = summed_rows + jnp.where((offset < window)[None, :], rows_back, 0.0)
    place = lax.axis_index("sp") * positions + jnp.arange(positions)
    count = jnp.minimum(place[:, None] + 1, window[None, :]).astype(jnp.float32)
    mixed = (summed_rows / count - pool32).astype(jnp.bfloat16)
    mapped = jnp.einsum(
        "tgc,gcd->tgd",
        mixed.reshape(positions, heads_dev, DK),
        pool_mix,
        preferred_element_type=jnp.float32,
    ).reshape(positions, head_cols)
    y_pool = (mapped * pool_gain[None, :] * jax.nn.silu(pgate.astype(jnp.float32))).astype(
        jnp.bfloat16
    )
    out_parts = (
        lax.all_gather(out_rec, "sp", axis=1, tiled=True),
        lax.all_gather(out_pool, "sp", axis=1, tiled=True),
    )
    both = jnp.concatenate([y_rec, y_pool], axis=1)
    weight_cat = jnp.concatenate(out_parts, axis=0)
    summed = lax.psum_scatter(
        jnp.dot(both, weight_cat, preferred_element_type=jnp.float32).astype(jnp.bfloat16),
        "tp",
        scatter_dimension=0,
        tiled=True,
    ).astype(jnp.float32)
    final = (
        summed
        * lax.rsqrt(jnp.mean(summed * summed, axis=1, keepdims=True) + eps)
        * post_gain[None, :]
    )
    return final.astype(jnp.bfloat16)


def solution(mesh):
    placed = (
        P("sp", "tp"),
        P(),
        P("sp", "tp"),
        P("sp", "tp"),
        P("sp", "tp"),
        P("sp", "tp"),
        P("sp", "tp"),
        P("sp", "tp"),
        P("tp"),
        P("sp", "tp"),
        P("tp"),
        P("tp", None, None),
        P("tp"),
        P("tp", "sp"),
        P("tp", "sp"),
        P(),
    )
    return jax.shard_map(
        per_device, mesh=mesh, in_specs=placed, out_specs=P(("sp", "tp"), None), check_vma=False
    )
```

profile of v0, /device:TPU:0, one launch (start us, length us, event | category | flops | bytes accessed | tf_op | source)
XLA Modules:
  0.0 518.1 jit_solution(14276728240443677830)
XLA Ops:
  6.5 0.7 all-gather.14.cloned.1.call-update
  7.3 0.7 all-gather.16.cloned.1.call-update
  10.5 0.7 all-gather.26.cloned.1.call-update
  11.3 0.8 copy.44
  12.1 0.7 exponential-minus-one_negate_fusion
  12.8 20.1 %all-gather.14.cloned.1.call-done = bf16[256,2048]{1,0:T(8,128)(2,1)} async-done(((bf16[256,1024]{1,0:T(8,128)(2,1)}), bf16[256,2048]{1,0:T(8,128)(2,1)}) %all-gather.14.cloned.1.call-update) | async-done | bytes 1048592 | tf_op jit(solution)/shard_map/all_gather | solution.py:104
  32.9 1.5 fusion.34
  34.4 42.1 %all-gather.16.cloned.1.call-done = bf16[2048,512]{1,0:T(8,128)(2,1)} async-done(((bf16[128,512]{1,0:T(8,128)(2,1)}), bf16[2048,512]{1,0:T(8,128)(2,1)}) %all-gather.16.cloned.1.call-update) | async-done | bytes 2097168 | tf_op jit(solution)/shard_map/all_gather | solution.py:93
  76.6 3.2 constant_dynamic-update-slice_fusion.5
  79.7 39.2 %all-gather.18.cloned.1.call-done = bf16[2048,512]{1,0:T(8,128)(2,1)} async-done(((bf16[128,512]{1,0:T(8,128)(2,1)}), bf16[2048,512]{1,0:T(8,128)(2,1)}) %all-gather.18.cloned.1.call-update) | async-done | bytes 2097168 | tf_op jit(solution)/shard_map/all_gather | solution.py:94
  118.9 3.2 constant_dynamic-update-slice_fusion.4
  122.2 39.0 %all-gather.20.cloned.1.call-done = bf16[2048,512]{1,0:T(8,128)(2,1)} async-done(((bf16[128,512]{1,0:T(8,128)(2,1)}), bf16[2048,512]{1,0:T(8,128)(2,1)}) %all-gather.20.cloned.1.call-update) | async-done | bytes 2097168 | tf_op jit(solution)/shard_map/all_gather | solution.py:95
  161.2 3.1 constant_dynamic-update-slice_fusion.3
  164.3 39.1 %all-gather.22.cloned.1.call-done = bf16[2048,512]{1,0:T(8,128)(2,1)} async-done(((bf16[128,512]{1,0:T(8,128)(2,1)}), bf16[2048,512]{1,0:T(8,128)(2,1)}) %all-gather.22.cloned.1.call-update) | async-done | bytes 2097168 | tf_op jit(solution)/shard_map/all_gather | solution.py:96
  203.4 3.2 constant_dynamic-update-slice_fusion.2
  206.6 39.0 %all-gather.24.cloned.1.call-done = bf16[2048,512]{1,0:T(8,128)(2,1)} async-done(((bf16[128,512]{1,0:T(8,128)(2,1)}), bf16[2048,512]{1,0:T(8,128)(2,1)}) %all-gather.24.cloned.1.call-update) | async-done | bytes 2097168 | tf_op jit(solution)/shard_map/all_gather | solution.py:97
  245.6 3.2 constant_dynamic-update-slice_fusion.1
  248.8 39.1 %all-gather.26.cloned.1.call-done = bf16[2048,512]{1,0:T(8,128)(2,1)} async-done(((bf16[128,512]{1,0:T(8,128)(2,1)}), bf16[2048,512]{1,0:T(8,128)(2,1)}) %all-gather.26.cloned.1.call-update) | async-done | bytes 2097168 | tf_op jit(solution)/shard_map/all_gather | solution.py:98
  288.0 3.1 constant_dynamic-update-slice_fusion
  291.1 8.0 %fusion.29 = bf16[256,3072]{1,0:T(8,128)(2,1)S(1)} fusion(bf16[2048,3072]{1,0:T(8,128)(2,1)} %constant_dynamic-update-slice_fusion, f32[256]{0:T(256)S(1)} %add_rsqrt_fusion.1, bf16[256,2048]{1,0:T(8,128)(2,1)S(1)} %copy-done.3, f32[2048]{0:T(1024)S(1)} %copy-done.10), kind=kOutput, calls=%fused_computation.44 | convolution fusion | flops 3224371200 | bytes 15213568 | tf_op jit(solution)/shard_map/dot_general | solution.py:106
  299.1 1.0 slice_convert_fusion.1
  301.9 48.2 %while.30 = (s32[]{:T(128)}, f32[4,128,128]{2,1,0:T(8,128)S(1)}, f32[4,128]{1,0:T(4,128)S(1)}, f32[4,4,64,128]{3,2,0,1:T(8,128)}, f32[4,4,64,128]{3,2,0,1:T(8,12...) while((s32[]{:T(128)}, f32[4,128,128]{2,1,0:T(8,128)S(1)}, ...), condition=%wide.region_3.4_spmd.clone, body=%wide.region_1.3_spmd.clone.sunk | while | flops 140923904 | bytes 20806288 | solution.py:68
  302.3 1.7 exponential_select_fusion.2
  304.0 7.3 %fusion.136 = f32[4,64,64]{1,2,0:T(8,128)S(1)} fusion(f32[4,64,64,128]{3,2,1,0:T(8,128)S(1)} %exponential_select_fusion.2, f32[4,128,64]{1,2,0:T(8,128)S(1)} %dynamic-slice_bitcast_fusion.9, f32[4,128,64]{1,2,0:T(8,128)S(1)} %get-tuple-element.298), kind=kLoop, calls=%fused_computation.4.clone.1 | loop fusion | flops 6275072 | bytes 8716288 | tf_op jit(solution)/shard_map/while/body/eval_jaxpr/htk,hsk,htsk->hts/dot_general | solution.py:52
  311.7 1.0 fusion.138
  314.3 1.7 exponential_select_fusion.2
  316.0 7.3 %fusion.136 = f32[4,64,64]{1,2,0:T(8,128)S(1)} fusion(f32[4,64,64,128]{3,2,1,0:T(8,128)S(1)} %exponential_select_fusion.2, f32[4,128,64]{1,2,0:T(8,128)S(1)} %dynamic-slice_bitcast_fusion.9, f32[4,128,64]{1,2,0:T(8,128)S(1)} %get-tuple-element.298), kind=kLoop, calls=%fused_computation.4.clone.1 | loop fusion | flops 6275072 | bytes 8716288 | tf_op jit(solution)/shard_map/while/body/eval_jaxpr/htk,hsk,htsk->hts/dot_general | solution.py:52
  323.7 1.0 fusion.138
  326.3 1.7 exponential_select_fusion.2
  328.0 7.3 %fusion.136 = f32[4,64,64]{1,2,0:T(8,128)S(1)} fusion(f32[4,64,64,128]{3,2,1,0:T(8,128)S(1)} %exponential_select_fusion.2, f32[4,128,64]{1,2,0:T(8,128)S(1)} %dynamic-slice_bitcast_fusion.9, f32[4,128,64]{1,2,0:T(8,128)S(1)} %get-tuple-element.298), kind=kLoop, calls=%fused_computation.4.clone.1 | loop fusion | flops 6275072 | bytes 8716288 | tf_op jit(solution)/shard_map/while/body/eval_jaxpr/htk,hsk,htsk->hts/dot_general | solution.py:52
  335.7 1.0 fusion.138
  338.3 1.7 exponential_select_fusion.2
  340.0 7.3 %fusion.136 = f32[4,64,64]{1,2,0:T(8,128)S(1)} fusion(f32[4,64,64,128]{3,2,1,0:T(8,128)S(1)} %exponential_select_fusion.2, f32[4,128,64]{1,2,0:T(8,128)S(1)} %dynamic-slice_bitcast_fusion.9, f32[4,128,64]{1,2,0:T(8,128)S(1)} %get-tuple-element.298), kind=kLoop, calls=%fused_computation.4.clone.1 | loop fusion | flops 6275072 | bytes 8716288 | tf_op jit(solution)/shard_map/while/body/eval_jaxpr/htk,hsk,htsk->hts/dot_general | solution.py:52
  347.7 1.0 fusion.138
  350.1 0.7 copy-done.1
  352.5 0.7 slice.99
  353.2 2.1 collective-permute-start
  355.4 19.7 %all-gather.2 = f32[16,4,128]{2,1,0:T(4,128)S(1)} all-gather(f32[1,4,128]{2,1,0:T(4,128)S(1)} %exponential_bitcast_fusion), channel_id=2, replica_groups=mesh['sp'=16,'tp'=2] {'sp'}, dimensions={0}, use_global_device_ids=true | all-gather | bytes 34816 | tf_op jit(solution)/shard_map/all_gather | solution.py:14
  375.1 1.7 fusion.103
  377.0 23.2 %all-gather.32.cloned.1.call-done = f32[64,128,128]{2,1,0:T(8,128)} async-done(((f32[4,128,128]{2,1,0:T(8,128)}), f32[64,128,128]{2,1,0:T(8,128)}) %all-gather.32.cloned.1.call-update) | async-done | bytes 4194320 | tf_op jit(solution)/shard_map/all_gather | solution.py:14
  400.3 0.7 multiply_reduce_fusion
  401.8 1.4 fusion.101
  403.2 38.8 %all-gather.28.cloned.1.call-done = bf16[512,2048]{1,0:T(8,128)(2,1)} async-done(((bf16[512,128]{1,0:T(8,128)(2,1)}), bf16[512,2048]{1,0:T(8,128)(2,1)}) %all-gather.28.cloned.1.call-update) | async-done | bytes 2097168 | tf_op jit(solution)/shard_map/all_gather | solution.py:173
  442.0 42.2 %all-gather.30.cloned.1.call-done = bf16[512,2048]{1,0:T(8,128)(2,1)} async-done(((bf16[512,128]{1,0:T(8,128)(2,1)}), bf16[512,2048]{1,0:T(8,128)(2,1)}) %all-gather.30.cloned.1.call-update) | async-done | bytes 2097168 | tf_op jit(solution)/shard_map/all_gather | solution.py:174
  484.1 4.5 fusion.30
  488.6 19.6 %reduce-scatter.2.cloned.1.call-done = bf16[128,2048]{1,0:T(8,128)(2,1)} async-done(((bf16[256,2048]{1,0:T(8,128)(2,1)}), bf16[128,2048]{1,0:T(8,128)(2,1)}) %reduce-scatter.2.cloned.1.call-update) | async-done | bytes 524304 | tf_op jit(solution)/shard_map/reduce_scatter | solution.py:178
  508.3 1.2 fusion.37
  509.5 2.0 fusion.39
  (110 shorter events, 14.6 us)
Async XLA Ops:
  6.5 368.5 %copy-start = (bf16[4,128,128]{2,1,0:T(8,128)(2,1)S(1)}, bf16[4,128,128]{2,1,0:T(8,128)(2,1)}, u32[]{:S(2)}) copy-start(bf16[4,128,128]{2,1,0:T(8,128)(2,1)} %param.31) | copy-start | bytes 393220
  6.5 26.4 %all-gather.14.cloned.1.call-start = ((), (), s32[]{:S(2)}) async-start(), calls=%async_computation.1 | async-start | bytes 1572864 | tf_op jit(solution)/shard_map/all_gather | solution.py:104
  7.3 69.3 %all-gather.16.cloned.1.call-start = ((), (), s32[]{:S(2)}) async-start(), calls=%async_computation.2 | async-start | bytes 2228224 | tf_op jit(solution)/shard_map/all_gather | solution.py:93
  8.0 110.9 %all-gather.18.cloned.1.call-start = ((), (), s32[]{:S(2)}) async-start(), calls=%async_computation.3 | async-start | bytes 2228224 | tf_op jit(solution)/shard_map/all_gather | solution.py:94
  8.7 152.4 %all-gather.20.cloned.1.call-start = ((), (), s32[]{:S(2)}) async-start(), calls=%async_computation.4 | async-start | bytes 2228224 | tf_op jit(solution)/shard_map/all_gather | solution.py:95
  9.3 194.1 %all-gather.22.cloned.1.call-start = ((), (), s32[]{:S(2)}) async-start(), calls=%async_computation.5 | async-start | bytes 2228224 | tf_op jit(solution)/shard_map/all_gather | solution.py:96
  9.9 235.7 %all-gather.24.cloned.1.call-start = ((), (), s32[]{:S(2)}) async-start(), calls=%async_computation.6 | async-start | bytes 2228224 | tf_op jit(solution)/shard_map/all_gather | solution.py:97
  10.5 277.5 %all-gather.26.cloned.1.call-start = ((), (), s32[]{:S(2)}) async-start(), calls=%async_computation.7 | async-start | bytes 2228224 | tf_op jit(solution)/shard_map/all_gather | solution.py:98
  11.2 389.0 %all-gather.32.cloned.1.call-start = ((), (), s32[]{:S(2)}) async-start(), calls=%async_computation.11 | async-start | bytes 4456448 | tf_op jit(solution)/shard_map/all_gather | solution.py:14
  206.6 84.5 %copy-start.3 = (bf16[256,2048]{1,0:T(8,128)(2,1)S(1)}, bf16[256,2048]{1,0:T(8,128)(2,1)}, u32[]{:S(2)}) copy-start(bf16[256,2048]{1,0:T(8,128)(2,1)} %all-gather.14.cloned.1.call-done) | copy-start | bytes 3145732
  206.6 84.5 %copy-start.10 = (f32[2048]{0:T(1024)S(1)}, f32[2048]{0:T(1024)}, u32[]{:S(2)}) copy-start(f32[2048]{0:T(1024)} %param.21) | copy-start | bytes 24580
  299.1 1.7 copy-start.2
  301.9 73.2 %copy-start.4 = (f32[256,512]{1,0:T(8,128)S(1)}, f32[256,512]{1,0:T(8,128)}, u32[]{:S(2)}) copy-start(f32[256,512]{1,0:T(8,128)} %get-tuple-element.180) | copy-start | bytes 1572868
  350.1 0.7 copy-start.1
  350.9 91.1 %all-gather.28.cloned.1.call-start = ((), (), s32[]{:S(2)}) async-start(), calls=%async_computation.8 | async-start | bytes 2228224 | tf_op jit(solution)/shard_map/all_gather | solution.py:173
  351.6 132.5 %all-gather.30.cloned.1.call-start = ((), (), s32[]{:S(2)}) async-start(), calls=%async_computation.9 | async-start | bytes 2228224 | tf_op jit(solution)/shard_map/all_gather | solution.py:174
  352.2 156.1 %reduce-scatter.2.cloned.1.call-start = ((), (), s32[]{:S(2)}) async-start(), calls=%async_computation.10 | async-start | bytes 1572864 | tf_op jit(solution)/shard_map/reduce_scatter | solution.py:178
  353.2 21.8 %collective-permute-start = (bf16[16,512]{1,0:T(8,128)(2,1)S(1)}, bf16[16,512]{1,0:T(8,128)(2,1)S(1)}, u32[]{:S(2)}, u32[]{:S(2)}) collective-permute-start(bf16[16,512]{1,0:T(8,128)(2,1)S(1)} %slice.99), channel_id=1, source_target_pairs={{0,2},{2,4},{4,6},{6,8},{8,10},{10,12},{12,14},{14,16},{16,18},{18... | collective-permute-start | bytes 49160 | tf_op jit(solution)/shard_map/ppermute | solution.py:28
  376.8 23.4 %copy-start.5 = (f32[4,4,64,128]{3,2,0,1:T(8,128)S(1)}, f32[4,4,64,128]{3,2,0,1:T(8,128)}, u32[]{:S(2)}) copy-start(f32[4,4,64,128]{3,2,0,1:T(8,128)} %get-tuple-element.104) | copy-start | bytes 1572868
  376.8 23.4 %copy-start.6 = (f32[4,4,64,128]{3,2,0,1:T(8,128)S(1)}, f32[4,4,64,128]{3,2,0,1:T(8,128)}, u32[]{:S(2)}) copy-start(f32[4,4,64,128]{3,2,0,1:T(8,128)} %get-tuple-element.108) | copy-start | bytes 1572868
  377.0 24.8 %copy-start.8 = (f32[512]{0:T(512)S(1)}, f32[512]{0:T(512)}, u32[]{:S(2)}) copy-start(f32[512]{0:T(512)} %param.30) | copy-start | bytes 6148
  377.0 24.8 %copy-start.9 = (f32[512]{0:T(512)S(1)}, f32[512]{0:T(512)}, u32[]{:S(2)}) copy-start(f32[512]{0:T(512)} %param.32) | copy-start | bytes 6148
  484.1 25.4 %copy-start.7 = (f32[2048]{0:T(1024)S(1)}, f32[2048]{0:T(1024)}, u32[]{:S(2)}) copy-start(f32[2048]{0:T(1024)} %param.35) | copy-start | bytes 24580
Sparse Core Ops, SparseCore 0:
  8.9 23.9 all-gather.13
  35.1 41.4 all-gather.15
  78.7 40.1 all-gather.17
  121.0 40.1 all-gather.19
  163.2 40.1 all-gather.21
  205.4 40.1 all-gather.23
  247.8 40.1 all-gather.25
  351.0 49.1 all-gather.31
  402.4 39.5 all-gather.27
  444.0 40.1 all-gather.29
  488.8 19.4 reduce-scatter.1
where the time goes:
time: 519 us; the launch traced here: 518 us
  waiting for transfers between devices  387 us (75%)
  other arithmetic  47.9 us (9%)
  local copies, waits for them, and re-layouts  23.9 us (5%)
  matrix products  23.2 us (4%)
  blocking collectives  19.7 us (4%)
  between operations  13.6 us (3%)
    all_gather x1, waiting for transfers between devices, per_device(): lax.all_gather(out_pool, 'sp', axis=1, tiled=True)  42.2 us
    all_gather x1, waiting for transfers between devices, per_device(): lax.all_gather(w_query, 'sp', axis=0, tiled=True)  42.1 us
    all_gather x1, waiting for transfers between devices, per_device(): lax.all_gather(w_forget, 'sp', axis=0, tiled=True)  39.2 us
    all_gather x1, waiting for transfers between devices, per_device(): lax.all_gather(w_pgate, 'sp', axis=0, tiled=True)  39.1 us
    all_gather x1, waiting for transfers between devices, per_device(): lax.all_gather(w_rgate, 'sp', axis=0, tiled=True)  39.1 us
    all_gather x1, waiting for transfers between devices, per_device(): lax.all_gather(w_pool_in, 'sp', axis=0, tiled=True)  39 us
    all_gather x1, waiting for transfers between devices, per_device(): lax.all_gather(w_input, 'sp', axis=0, tiled=True)  39 us
    all_gather x1, waiting for transfers between devices, per_device(): lax.all_gather(out_rec, 'sp', axis=1, tiled=True)  38.8 us
  transfers between devices with their start and end apart: 12, of which 11 were waited for; matrix products, arithmetic and copies ran while one was open for 5% of the time, Pallas kernels for 0%

commit v1 on v0

--- a/solution.py
+++ b/solution.py
@@ -170,7 +170,7 @@
         jnp.bfloat16
     )
     out_parts = (
-        lax.all_gather(out_rec, "sp", axis=1, tiled=True),
+        jnp.concatenate(lax.all_gather(out_rec, "sp"), axis=1),
         lax.all_gather(out_pool, "sp", axis=1, tiled=True),
     )
     both = jnp.concatenate([y_rec, y_pool], axis=1)

time: 519 us -> 476 us (0.917)
  waiting for transfers between devices: 387 us -> 340 us
    all_gather x1, waiting for transfers between devices: 38.8 us -> 0.02 us  [per_device(): lax.all_gather(out_rec, 'sp')]
    unnamed x29 -> x26, local copies, waits for them, and re-layouts: 17.6 us -> 18 us
  transfers between devices with their start and end apart: 12 -> 12, of which waited for: 11 -> 10; matrix products, arithmetic and copies ran while one was open for 5% -> 19% of each run, Pallas kernels for 0% -> 0%
where the time goes in v1:
time: 476 us; the launch traced here: 475 us
  waiting for transfers between devices  340 us (71%)
  other arithmetic  47.9 us (10%)
  local copies, waits for them, and re-layouts  27.5 us (6%)
  matrix products  23.8 us (5%)
  blocking collectives  19.4 us (4%)
  between operations  13.5 us (3%)
    all_gather x1, waiting for transfers between devices, per_device(): lax.all_gather(w_query, 'sp', axis=0, tiled=True)  42.1 us
    all_gather x1, waiting for transfers between devices, per_device(): lax.all_gather(w_forget, 'sp', axis=0, tiled=True)  39.2 us
    all_gather x1, waiting for transfers between devices, per_device(): lax.all_gather(w_pgate, 'sp', axis=0, tiled=True)  39.2 us
    all_gather x1, waiting for transfers between devices, per_device(): lax.all_gather(w_pool_in, 'sp', axis=0, tiled=True)  39.1 us
    all_gather x1, waiting for transfers between devices, per_device(): lax.all_gather(w_input, 'sp', axis=0, tiled=True)  39 us
    all_gather x1, waiting for transfers between devices, per_device(): lax.all_gather(w_rgate, 'sp', axis=0, tiled=True)  39 us
    all_gather x1, waiting for transfers between devices, per_device(): lax.all_gather(out_pool, 'sp', axis=1, tiled=True)  37.4 us
    dot_general x4, other arithmetic, advance(): jnp.einsum('htk,hsk,htsk->hts', probe_segment, key_piece, weight, precisi...  29.3 us
  transfers between devices with their start and end apart: 12, of which 10 were waited for; matrix products, arithmetic and copies ran while one was open for 19% of the time, Pallas kernels for 0%

profile of v1, /device:TPU:0, one launch (start us, length us, event | category | flops | bytes accessed | tf_op | source)
XLA Modules:
  0.0 475.2 jit_solution(4810586418535087580)
XLA Ops:
  6.5 0.7 all-gather.15.cloned.1.call-update
  7.3 0.7 all-gather.17.cloned.1.call-update
  10.5 0.7 all-gather.27.cloned.1.call-update
  11.3 0.7 all-gather.33.cloned.1.call-update
  12.1 0.8 copy.46
  13.6 19.3 %all-gather.15.cloned.1.call-done = bf16[256,2048]{1,0:T(8,128)(2,1)} async-done(((bf16[256,1024]{1,0:T(8,128)(2,1)}), bf16[256,2048]{1,0:T(8,128)(2,1)}) %all-gather.15.cloned.1.call-update) | async-done | bytes 1048592 | tf_op jit(solution)/shard_map/all_gather | solution.py:104
  32.9 1.5 fusion.34
  34.4 42.1 %all-gather.17.cloned.1.call-done = bf16[2048,512]{1,0:T(8,128)(2,1)} async-done(((bf16[128,512]{1,0:T(8,128)(2,1)}), bf16[2048,512]{1,0:T(8,128)(2,1)}) %all-gather.17.cloned.1.call-update) | async-done | bytes 2097168 | tf_op jit(solution)/shard_map/all_gather | solution.py:93
  76.6 3.1 constant_dynamic-update-slice_fusion.5
  79.7 39.2 %all-gather.19.cloned.1.call-done = bf16[2048,512]{1,0:T(8,128)(2,1)} async-done(((bf16[128,512]{1,0:T(8,128)(2,1)}), bf16[2048,512]{1,0:T(8,128)(2,1)}) %all-gather.19.cloned.1.call-update) | async-done | bytes 2097168 | tf_op jit(solution)/shard_map/all_gather | solution.py:94
  118.9 3.2 constant_dynamic-update-slice_fusion.4
  122.1 39.0 %all-gather.21.cloned.1.call-done = bf16[2048,512]{1,0:T(8,128)(2,1)} async-done(((bf16[128,512]{1,0:T(8,128)(2,1)}), bf16[2048,512]{1,0:T(8,128)(2,1)}) %all-gather.21.cloned.1.call-update) | async-done | bytes 2097168 | tf_op jit(solution)/shard_map/all_gather | solution.py:95
  161.2 3.2 constant_dynamic-update-slice_fusion.3
  164.4 39.0 %all-gather.23.cloned.1.call-done = bf16[2048,512]{1,0:T(8,128)(2,1)} async-done(((bf16[128,512]{1,0:T(8,128)(2,1)}), bf16[2048,512]{1,0:T(8,128)(2,1)}) %all-gather.23.cloned.1.call-update) | async-done | bytes 2097168 | tf_op jit(solution)/shard_map/all_gather | solution.py:96
  203.4 3.1 constant_dynamic-update-slice_fusion.2
  206.5 39.1 %all-gather.25.cloned.1.call-done = bf16[2048,512]{1,0:T(8,128)(2,1)} async-done(((bf16[128,512]{1,0:T(8,128)(2,1)}), bf16[2048,512]{1,0:T(8,128)(2,1)}) %all-gather.25.cloned.1.call-update) | async-done | bytes 2097168 | tf_op jit(solution)/shard_map/all_gather | solution.py:97
  245.6 3.2 constant_dynamic-update-slice_fusion.1
  248.8 39.2 %all-gather.27.cloned.1.call-done = bf16[2048,512]{1,0:T(8,128)(2,1)} async-done(((bf16[128,512]{1,0:T(8,128)(2,1)}), bf16[2048,512]{1,0:T(8,128)(2,1)}) %all-gather.27.cloned.1.call-update) | async-done | bytes 2097168 | tf_op jit(solution)/shard_map/all_gather | solution.py:98
  288.0 3.2 constant_dynamic-update-slice_fusion
  291.2 8.0 %fusion.29 = bf16[256,3072]{1,0:T(8,128)(2,1)S(1)} fusion(bf16[2048,3072]{1,0:T(8,128)(2,1)} %constant_dynamic-update-slice_fusion, f32[256]{0:T(256)S(1)} %add_rsqrt_fusion.1, bf16[256,2048]{1,0:T(8,128)(2,1)S(1)} %copy-done.3, f32[2048]{0:T(1024)S(1)} %copy-done.8), kind=kOutput, calls=%fused_computation.44 | convolution fusion | flops 3224371200 | bytes 15213568 | tf_op jit(solution)/shard_map/dot_general | solution.py:106
  299.2 1.0 slice_convert_fusion.1
  302.0 48.3 %while.30 = (s32[]{:T(128)}, f32[4,128,128]{2,1,0:T(8,128)S(1)}, f32[4,128]{1,0:T(4,128)S(1)}, f32[4,4,64,128]{3,2,0,1:T(8,128)}, f32[4,4,64,128]{3,2,0,1:T(8,12...) while((s32[]{:T(128)}, f32[4,128,128]{2,1,0:T(8,128)S(1)}, ...), condition=%wide.region_3.4_spmd.clone, body=%wide.region_1.3_spmd.clone.sunk | while | flops 140923904 | bytes 20806288 | solution.py:68
  302.4 1.7 exponential_select_fusion.2
  304.1 7.3 %fusion.136 = f32[4,64,64]{1,2,0:T(8,128)S(1)} fusion(f32[4,64,64,128]{3,2,1,0:T(8,128)S(1)} %exponential_select_fusion.2, f32[4,128,64]{1,2,0:T(8,128)S(1)} %dynamic-slice_bitcast_fusion.9, f32[4,128,64]{1,2,0:T(8,128)S(1)} %get-tuple-element.298), kind=kLoop, calls=%fused_computation.4.clone.1 | loop fusion | flops 6275072 | bytes 8716288 | tf_op jit(solution)/shard_map/while/body/eval_jaxpr/htk,hsk,htsk->hts/dot_general | solution.py:52
  311.8 1.0 fusion.138
  314.4 1.7 exponential_select_fusion.2
  316.1 7.3 %fusion.136 = f32[4,64,64]{1,2,0:T(8,128)S(1)} fusion(f32[4,64,64,128]{3,2,1,0:T(8,128)S(1)} %exponential_select_fusion.2, f32[4,128,64]{1,2,0:T(8,128)S(1)} %dynamic-slice_bitcast_fusion.9, f32[4,128,64]{1,2,0:T(8,128)S(1)} %get-tuple-element.298), kind=kLoop, calls=%fused_computation.4.clone.1 | loop fusion | flops 6275072 | bytes 8716288 | tf_op jit(solution)/shard_map/while/body/eval_jaxpr/htk,hsk,htsk->hts/dot_general | solution.py:52
  323.8 1.0 fusion.138
  326.4 1.7 exponential_select_fusion.2
  328.1 7.3 %fusion.136 = f32[4,64,64]{1,2,0:T(8,128)S(1)} fusion(f32[4,64,64,128]{3,2,1,0:T(8,128)S(1)} %exponential_select_fusion.2, f32[4,128,64]{1,2,0:T(8,128)S(1)} %dynamic-slice_bitcast_fusion.9, f32[4,128,64]{1,2,0:T(8,128)S(1)} %get-tuple-element.298), kind=kLoop, calls=%fused_computation.4.clone.1 | loop fusion | flops 6275072 | bytes 8716288 | tf_op jit(solution)/shard_map/while/body/eval_jaxpr/htk,hsk,htsk->hts/dot_general | solution.py:52
  335.8 1.0 fusion.138
  338.4 1.7 exponential_select_fusion.2
  340.1 7.3 %fusion.136 = f32[4,64,64]{1,2,0:T(8,128)S(1)} fusion(f32[4,64,64,128]{3,2,1,0:T(8,128)S(1)} %exponential_select_fusion.2, f32[4,128,64]{1,2,0:T(8,128)S(1)} %dynamic-slice_bitcast_fusion.9, f32[4,128,64]{1,2,0:T(8,128)S(1)} %get-tuple-element.298), kind=kLoop, calls=%fused_computation.4.clone.1 | loop fusion | flops 6275072 | bytes 8716288 | tf_op jit(solution)/shard_map/while/body/eval_jaxpr/htk,hsk,htsk->hts/dot_general | solution.py:52
  347.8 1.0 fusion.138
  350.2 0.7 copy-done.1
  351.9 0.7 slice.99
  352.6 2.3 collective-permute-start
  355.0 3.0 copy.58
  358.5 19.4 %all-gather.3 = f32[16,4,128]{2,1,0:T(4,128)S(1)} all-gather(f32[1,4,128]{2,1,0:T(4,128)S(1)} %exponential_bitcast_fusion), channel_id=2, replica_groups=mesh['sp'=16,'tp'=2] {'sp'}, dimensions={0}, use_global_device_ids=true | all-gather | bytes 34816 | tf_op jit(solution)/shard_map/all_gather | solution.py:14
  377.9 1.7 fusion.103
  379.9 20.4 %all-gather.31.cloned.1.call-done = f32[64,128,128]{2,1,0:T(8,128)} async-done(((f32[4,128,128]{2,1,0:T(8,128)}), f32[64,128,128]{2,1,0:T(8,128)}) %all-gather.31.cloned.1.call-update) | async-done | bytes 4194320 | tf_op jit(solution)/shard_map/all_gather | solution.py:14
  400.3 1.9 multiply_reduce_fusion
  403.1 1.4 fusion.101
  404.5 37.4 %all-gather.29.cloned.1.call-done = bf16[512,2048]{1,0:T(8,128)(2,1)} async-done(((bf16[512,128]{1,0:T(8,128)(2,1)}), bf16[512,2048]{1,0:T(8,128)(2,1)}) %all-gather.29.cloned.1.call-update) | async-done | bytes 2097168 | tf_op jit(solution)/shard_map/all_gather | solution.py:174
  441.9 3.8 fusion.30
  445.8 19.6 %reduce-scatter.2.cloned.1.call-done = bf16[128,2048]{1,0:T(8,128)(2,1)} async-done(((bf16[256,2048]{1,0:T(8,128)(2,1)}), bf16[128,2048]{1,0:T(8,128)(2,1)}) %reduce-scatter.2.cloned.1.call-update) | async-done | bytes 524304 | tf_op jit(solution)/shard_map/reduce_scatter | solution.py:178
  465.4 1.2 fusion.37
  466.7 2.0 fusion.39
  (108 shorter events, 15.2 us)
Async XLA Ops:
  6.5 371.4 %copy-start = (bf16[4,128,128]{2,1,0:T(8,128)(2,1)S(1)}, bf16[4,128,128]{2,1,0:T(8,128)(2,1)}, u32[]{:S(2)}) copy-start(bf16[4,128,128]{2,1,0:T(8,128)(2,1)} %param.31) | copy-start | bytes 393220
  6.5 26.4 %all-gather.15.cloned.1.call-start = ((), (), s32[]{:S(2)}) async-start(), calls=%async_computation.1 | async-start | bytes 1572864 | tf_op jit(solution)/shard_map/all_gather | solution.py:104
  7.3 69.3 %all-gather.17.cloned.1.call-start = ((), (), s32[]{:S(2)}) async-start(), calls=%async_computation.2 | async-start | bytes 2228224 | tf_op jit(solution)/shard_map/all_gather | solution.py:93
  8.0 110.9 %all-gather.19.cloned.1.call-start = ((), (), s32[]{:S(2)}) async-start(), calls=%async_computation.3 | async-start | bytes 2228224 | tf_op jit(solution)/shard_map/all_gather | solution.py:94
  8.7 152.4 %all-gather.21.cloned.1.call-start = ((), (), s32[]{:S(2)}) async-start(), calls=%async_computation.4 | async-start | bytes 2228224 | tf_op jit(solution)/shard_map/all_gather | solution.py:95
  9.3 194.1 %all-gather.23.cloned.1.call-start = ((), (), s32[]{:S(2)}) async-start(), calls=%async_computation.5 | async-start | bytes 2228224 | tf_op jit(solution)/shard_map/all_gather | solution.py:96
  9.9 235.7 %all-gather.25.cloned.1.call-start = ((), (), s32[]{:S(2)}) async-start(), calls=%async_computation.6 | async-start | bytes 2228224 | tf_op jit(solution)/shard_map/all_gather | solution.py:97
  10.5 277.5 %all-gather.27.cloned.1.call-start = ((), (), s32[]{:S(2)}) async-start(), calls=%async_computation.7 | async-start | bytes 2228224 | tf_op jit(solution)/shard_map/all_gather | solution.py:98
  11.2 343.7 %all-gather.33.cloned.1.call-start = ((), (), s32[]{:S(2)}) async-start(), calls=%async_computation.11 | async-start | bytes 2228224 | tf_op jit(solution)/shard_map/all_gather | solution.py:173
  12.0 388.3 %all-gather.31.cloned.1.call-start = ((), (), s32[]{:S(2)}) async-start(), calls=%async_computation.10 | async-start | bytes 4456448 | tf_op jit(solution)/shard_map/all_gather | solution.py:14
  206.5 84.7 %copy-start.3 = (bf16[256,2048]{1,0:T(8,128)(2,1)S(1)}, bf16[256,2048]{1,0:T(8,128)(2,1)}, u32[]{:S(2)}) copy-start(bf16[256,2048]{1,0:T(8,128)(2,1)} %all-gather.15.cloned.1.call-done) | copy-start | bytes 3145732
  206.5 84.7 %copy-start.8 = (f32[2048]{0:T(1024)S(1)}, f32[2048]{0:T(1024)}, u32[]{:S(2)}) copy-start(f32[2048]{0:T(1024)} %param.21) | copy-start | bytes 24580
  299.2 1.7 copy-start.2
  350.2 0.7 copy-start.1
  351.0 90.9 %all-gather.29.cloned.1.call-start = ((), (), s32[]{:S(2)}) async-start(), calls=%async_computation.8 | async-start | bytes 2228224 | tf_op jit(solution)/shard_map/all_gather | solution.py:174
  351.6 113.8 %reduce-scatter.2.cloned.1.call-start = ((), (), s32[]{:S(2)}) async-start(), calls=%async_computation.9 | async-start | bytes 1572864 | tf_op jit(solution)/shard_map/reduce_scatter | solution.py:178
  352.6 25.3 %collective-permute-start = (bf16[16,512]{1,0:T(8,128)(2,1)S(1)}, bf16[16,512]{1,0:T(8,128)(2,1)S(1)}, u32[]{:S(2)}, u32[]{:S(2)}) collective-permute-start(bf16[16,512]{1,0:T(8,128)(2,1)S(1)} %slice.99), channel_id=1, source_target_pairs={{0,2},{2,4},{4,6},{6,8},{8,10},{10,12},{12,14},{14,16},{16,18},{18... | collective-permute-start | bytes 49160 | tf_op jit(solution)/shard_map/ppermute | solution.py:28
  355.0 23.0 %copy-start.4 = (f32[256,512]{1,0:T(8,128)S(1)}, f32[256,512]{1,0:T(8,128)}, u32[]{:S(2)}) copy-start(f32[256,512]{1,0:T(8,128)} %get-tuple-element.180) | copy-start | bytes 1572868
  379.9 23.2 %copy-start.6 = (f32[512]{0:T(512)S(1)}, f32[512]{0:T(512)}, u32[]{:S(2)}) copy-start(f32[512]{0:T(512)} %param.30) | copy-start | bytes 6148
  379.9 23.2 %copy-start.7 = (f32[512]{0:T(512)S(1)}, f32[512]{0:T(512)}, u32[]{:S(2)}) copy-start(f32[512]{0:T(512)} %param.32) | copy-start | bytes 6148
  441.9 24.8 %copy-start.5 = (f32[2048]{0:T(1024)S(1)}, f32[2048]{0:T(1024)}, u32[]{:S(2)}) copy-start(f32[2048]{0:T(1024)} %param.35) | copy-start | bytes 24580
Sparse Core Ops, SparseCore 0:
  8.9 23.9 all-gather.14
  35.1 41.4 all-gather.16
  78.7 40.1 all-gather.18
  121.0 40.1 all-gather.20
  163.2 40.1 all-gather.22
  205.4 40.1 all-gather.24
  247.8 40.1 all-gather.26
  290.1 40.1 all-gather.32
  351.1 49.1 all-gather.30
  402.3 39.5 all-gather.28
  445.9 19.4 reduce-scatter.1
